TPU v7x, 32 devices: a whole 2x2x4 slice. The times are simulated.
32 devices in a mesh: rep: 1, fs: 8 (over z, y), tp: 4 (over x, core).
Axes of the slice: x: 2, y: 2, z: 4, core: 2. Of those that a mesh axis runs over, the one named last changes fastest.
Arguments:
- tokens: bfloat16 [4096, 2048], P(('rep', 'fs')), may hold values from -6 to 6
- gate_outer: bfloat16 [2048, 1024], P('fs', 'tp'), may hold values from -0.125 to 0.125
- gate_inner: bfloat16 [2048, 1024], P('fs', 'tp'), may hold values from -0.125 to 0.125
- conv_input: bfloat16 [2048, 1024], P('fs', 'tp'), may hold values from -0.125 to 0.125
- mixer_output: bfloat16 [2048, 1024], P('fs', 'tp'), may hold values from -0.1875 to 0.1875
- conv_taps: float32 [3, 1024], P(None, 'tp'), may hold values from -3 to 3
- mixer_gain: float32 [2048], replicated, may hold values from 0.1 to 1.9
- mixer_shift: float32 [2048], replicated, may hold values from -3 to 3
- up_weight: bfloat16 [2048, 8192], P('fs', 'tp'), may hold values from -0.125 to 0.125
- down_weight: bfloat16 [2048, 8192], P('fs', 'tp'), may hold values from -0.0625 to 0.0625
- channel_gain: float32 [2048], replicated, may hold values from 0.1 to 1.9
- channel_shift: float32 [2048], replicated, may hold values from -3 to 3
Outputs:
- mixed: bfloat16 [4096, 2048], P(('rep', 'fs'))
All inputs are finite; a program needn't handle non-finite values.
Results may differ from a plain program's by a relative error of at most 0.014.
Values may be sent and summed in bfloat16 or wider, within the bound.
A program may use at most 64 MiB of HBM per device.

v0:
```python
import jax
import jax.numpy as jnp
from jax import lax
from jax.sharding import PartitionSpec as P

residual_scale = 8.0**0.25
norm_epsilon = 1e-05


def layer_norm(values, gain, shift):
    row_mean = jnp.mean(values, -1, keepdims=True)
    centered = values - row_mean
    variance = jnp.mean(centered * centered, -1, keepdims=True)
    return centered * lax.rsqrt(variance + norm_epsilon) * gain + shift


def rounded_partial(left, right_t):
    product = lax.dot_general(
        left, right_t, (((1,), (1,)), ((), ())), preferred_element_type=jnp.float32
    )
    return lax.optimization_barrier(product.astype(jnp.bfloat16)).astype(jnp.float32)


def gated_conv(outer_gate, inner_gate, conv_values, conv_taps):
    seq_len = conv_values.shape[0]
    tap_count = conv_taps.shape[0]
    product = inner_gate * conv_values
    padded = jnp.pad(product, ((tap_count - 1, 0), (0, 0)))
    result = jnp.zeros_like(product)
    for tap_index in range(tap_count):
        result = result + conv_taps[tap_index] * padded[tap_index : tap_index + seq_len]
    return (outer_gate * result).astype(jnp.bfloat16)


def local(
    tokens,
    gate_outer,
    gate_inner,
    conv_input,
    mixer_output,
    conv_taps,
    mixer_gain,
    mixer_shift,
    up_weight,
    down_weight,
    channel_gain,
    channel_shift,
):
    seq_len = tokens.shape[0]
    own_rows = seq_len // lax.axis_size("tp")
    own_start = lax.axis_index("tp") * own_rows
    columns = tokens
    outer_gate = jnp.dot(
        columns,
        lax.all_gather(gate_outer, "fs", axis=0, tiled=True),
        preferred_element_type=jnp.float32,
    )
    inner_gate = jnp.dot(
        columns,
        lax.all_gather(gate_inner, "fs", axis=0, tiled=True),
        preferred_element_type=jnp.float32,
    )
    conv_values = jnp.dot(
        columns,
        lax.all_gather(conv_input, "fs", axis=0, tiled=True),
        preferred_element_type=jnp.float32,
    )
    output_weight = lax.all_gather(mixer_output, "fs", axis=0, tiled=True)
    conv_out = gated_conv(outer_gate, inner_gate, conv_values, conv_taps)
    mixer_sum = lax.psum(
        rounded_partial(conv_out, output_weight).astype(jnp.bfloat16), "tp"
    ).astype(jnp.float32)
    first_rows = layer_norm(
        residual_scale * tokens.astype(jnp.float32) + mixer_sum, mixer_gain, mixer_shift
    ).astype(jnp.bfloat16)
    first_own = lax.dynamic_slice_in_dim(first_rows, own_start, own_rows, 0)
    columns = first_rows
    up_product = jnp.dot(
        columns,
        lax.all_gather(up_weight, "fs", axis=0, tiled=True),
        preferred_element_type=jnp.float32,
    )
    down_full = lax.all_gather(down_weight, "fs", axis=0, tiled=True)
    hidden = jnp.square(jax.nn.relu(up_product)).astype(jnp.bfloat16)
    channel_sum = lax.psum_scatter(
        rounded_partial(hidden, down_full).astype(jnp.bfloat16),
        "tp",
        scatter_dimension=0,
        tiled=True,
    ).astype(jnp.float32)
    output_own = layer_norm(
        residual_scale * first_own.astype(jnp.float32) + channel_sum, channel_gain, channel_shift
    ).astype(jnp.bfloat16)
    return lax.all_gather(output_own, "tp", axis=0, tiled=True)


def solution(mesh):
    in_specs = (
        P(("rep", "fs"), None),
        P("fs", "tp"),
        P("fs", "tp"),
        P("fs", "tp"),
        P("fs", "tp"),
        P(None, "tp"),
        P(),
        P(),
        P("fs", "tp"),
        P("fs", "tp"),
        P(),
        P(),
    )
    out_specs = P(("rep", "fs"), None)
    return jax.shard_map(local, mesh=mesh, in_specs=in_specs, out_specs=out_specs, check_vma=False)
```

profile of v0, /device:TPU:0, one launch (start us, length us, event | category | flops | bytes accessed | tf_op | source)
XLA Modules:
  0.0 565.9 jit_solution(9245024707025191946)
XLA Ops:
  6.5 0.7 all-gather.10.cloned.1.call-update
  7.3 0.7 all-gather.12.cloned.1.call-update
  8.0 0.0 all-gather.14.cloned.1.call-start
  8.1 0.7 all-gather.14.cloned.1.call-update
  8.8 0.5 all-gather.8.cloned.1.call-update
  9.3 0.0 all-reduce.3.cloned.1.call-start
  9.4 0.8 fusion.16
  10.2 42.3 %all-gather.10.cloned.1.call-done = bf16[2048,256]{1,0:T(8,128)(2,1)} async-done(((bf16[256,256]{1,0:T(8,128)(2,1)}), bf16[2048,256]{1,0:T(8,128)(2,1)}) %all-gather.10.cloned.1.call-update) | async-done | bytes 1048592 | tf_op jit(solution)/shard_map/all_gather | solution.py:60
  52.5 2.6 fusion.17
  55.1 38.6 %all-gather.12.cloned.1.call-done = bf16[2048,256]{1,0:T(8,128)(2,1)} async-done(((bf16[256,256]{1,0:T(8,128)(2,1)}), bf16[2048,256]{1,0:T(8,128)(2,1)}) %all-gather.12.cloned.1.call-update) | async-done | bytes 1048592 | tf_op jit(solution)/shard_map/all_gather | solution.py:65
  93.6 1.9 convolution_multiply_fusion
  95.6 39.2 %all-gather.14.cloned.1.call-done = bf16[2048,256]{1,0:T(8,128)(2,1)} async-done(((bf16[256,256]{1,0:T(8,128)(2,1)}), bf16[2048,256]{1,0:T(8,128)(2,1)}) %all-gather.14.cloned.1.call-update) | async-done | bytes 1048592 | tf_op jit(solution)/shard_map/all_gather | solution.py:68
  134.8 41.0 %all-gather.8.cloned.1.call-done = bf16[2048,256]{1,0:T(8,128)(2,1)} async-done(((bf16[256,256]{1,0:T(8,128)(2,1)}), bf16[2048,256]{1,0:T(8,128)(2,1)}) %all-gather.8.cloned.1.call-update) | async-done | bytes 1048592 | tf_op jit(solution)/shard_map/all_gather | solution.py:55
  175.8 5.2 convolution_convert_fusion
  181.0 0.0 all-gather.16.cloned.1.call-start
  181.0 0.5 all-gather.16.cloned.1.call-update
  181.6 0.7 all-gather.18.cloned.1.call-update
  182.3 0.2 reduce-scatter.2.cloned.1.call-start
  182.6 48.7 %all-reduce.3.cloned.1.call-done = bf16[512,2048]{1,0:T(8,128)(2,1)} async-done(((bf16[512,2048]{1,0:T(8,128)(2,1)}), bf16[512,2048]{1,0:T(8,128)(2,1)}) %all-reduce.3.cloned.1.call-update) | async-done | bytes 2097168 | tf_op jit(solution)/shard_map/psum | solution.py:70
  231.2 2.5 fusion
  233.7 1.0 multiply_reduce_fusion
  234.8 2.5 add_convert_fusion
  237.3 120.5 %all-gather.16.cloned.1.call-done = bf16[2048,2048]{1,0:T(8,128)(2,1)} async-done(((bf16[256,2048]{1,0:T(8,128)(2,1)}), bf16[2048,2048]{1,0:T(8,128)(2,1)}) %all-gather.16.cloned.1.call-update) | async-done | bytes 8388624 | tf_op jit(solution)/shard_map/all_gather | solution.py:80
  357.8 124.8 %all-gather.18.cloned.1.call-done = bf16[2048,2048]{1,0:T(8,128)(2,1)} async-done(((bf16[256,2048]{1,0:T(8,128)(2,1)}), bf16[2048,2048]{1,0:T(8,128)(2,1)}) %all-gather.18.cloned.1.call-update) | async-done | bytes 8388624 | tf_op jit(solution)/shard_map/all_gather | solution.py:83
  482.6 16.5 %convolution_convert_fusion.1 = bf16[512,2048]{1,0:T(8,128)(2,1)} fusion(bf16[2048,2048]{1,0:T(8,128)(2,1)} %all-gather.18.cloned.1.call-done, bf16[512,2048]{1,0:T(8,128)(2,1)} %add_convert_fusion, bf16[2048,2048]{1,0:T(8,128)(2,1)} %all-gather.16.cloned.1.call-done), kind=kOutput, calls=%fused_computation.6 | convolution fusion | flops 8594128896 | bytes 20971520 | tf_op jit(solution)/shard_map/dot_general | solution.py:18
  499.2 0.0 all-gather.20.cloned.1.call-start
  499.2 29.4 %reduce-scatter.2.cloned.1.call-done = bf16[128,2048]{1,0:T(8,128)(2,1)} async-done(((bf16[512,2048]{1,0:T(8,128)(2,1)}), bf16[128,2048]{1,0:T(8,128)(2,1)}) %reduce-scatter.2.cloned.1.call-update) | async-done | bytes 524304 | tf_op jit(solution)/shard_map/reduce_scatter | solution.py:85
  528.6 1.3 fusion.2
  529.9 1.4 multiply_reduce_fusion.1
  531.3 2.2 add_convert_fusion.1
  533.5 22.7 %all-gather.20.cloned.1.call-done = bf16[512,2048]{1,0:T(8,128)(2,1)} async-done(((bf16[128,2048]{1,0:T(8,128)(2,1)}), bf16[512,2048]{1,0:T(8,128)(2,1)}) %all-gather.20.cloned.1.call-update) | async-done | bytes 2097168 | tf_op jit(solution)/shard_map/all_gather | solution.py:94
  556.3 3.2 copy.15
  (25 shorter events, 0.2 us)
Async XLA Ops:
  6.5 87.1 %copy-start = (bf16[512,2048]{1,0:T(8,128)(2,1)S(1)}, bf16[512,2048]{1,0:T(8,128)(2,1)}, u32[]{:S(2)}) copy-start(bf16[512,2048]{1,0:T(8,128)(2,1)} %param.12) | copy-start | bytes 6291460
  6.5 46.0 %all-gather.10.cloned.1.call-start = ((), (), s32[]{:S(2)}) async-start(), calls=%async_computation.2 | async-start | bytes 1179648 | tf_op jit(solution)/shard_map/all_gather | solution.py:60
  7.3 86.4 %all-gather.12.cloned.1.call-start = ((), (), s32[]{:S(2)}) async-start(), calls=%async_computation.3 | async-start | bytes 1179648 | tf_op jit(solution)/shard_map/all_gather | solution.py:65
  8.0 126.8 %all-gather.14.cloned.1.call-start = ((), (), s32[]{:S(2)}) async-start(), calls=%async_computation.4 | async-start | bytes 1179648 | tf_op jit(solution)/shard_map/all_gather | solution.py:68
  8.7 167.1 %all-gather.8.cloned.1.call-start = ((), (), s32[]{:S(2)}) async-start(), calls=%async_computation.1 | async-start | bytes 1179648 | tf_op jit(solution)/shard_map/all_gather | solution.py:55
  9.3 221.9 %all-reduce.3.cloned.1.call-start = ((), (), s32[]{:S(2)}) async-start(), calls=%async_computation.5 | async-start | bytes 4194304 | tf_op jit(solution)/shard_map/psum | solution.py:70
  181.0 176.8 %all-gather.16.cloned.1.call-start = ((), (), s32[]{:S(2)}) async-start(), calls=%async_computation.6 | async-start | bytes 9437184 | tf_op jit(solution)/shard_map/all_gather | solution.py:80
  181.6 301.0 %all-gather.18.cloned.1.call-start = ((), (), s32[]{:S(2)}) async-start(), calls=%async_computation.7 | async-start | bytes 9437184 | tf_op jit(solution)/shard_map/all_gather | solution.py:83
  182.3 52.4 %copy-start.3 = (f32[2048]{0:T(1024)S(1)}, f32[2048]{0:T(1024)}, u32[]{:S(2)}) copy-start(f32[2048]{0:T(1024)} %param.19) | copy-start | bytes 24580
  182.3 52.4 %copy-start.4 = (f32[2048]{0:T(1024)S(1)}, f32[2048]{0:T(1024)}, u32[]{:S(2)}) copy-start(f32[2048]{0:T(1024)} %param.18) | copy-start | bytes 24580
  182.3 346.3 %reduce-scatter.2.cloned.1.call-start = ((), (), s32[]{:S(2)}) async-start(), calls=%async_computation.8 | async-start | bytes 2621440 | tf_op jit(solution)/shard_map/reduce_scatter | solution.py:85
  231.2 2.5 copy-start.1
  237.3 291.4 %copy-start.2 = (bf16[512,2048]{1,0:T(8,128)(2,1)S(1)}, bf16[512,2048]{1,0:T(8,128)(2,1)}, u32[]{:S(2)}) copy-start(bf16[512,2048]{1,0:T(8,128)(2,1)} %add_convert_fusion) | copy-start | bytes 6291460
  499.1 32.2 %copy-start.5 = (f32[2048]{0:T(1024)S(1)}, f32[2048]{0:T(1024)}, u32[]{:S(2)}) copy-start(f32[2048]{0:T(1024)} %param.23) | copy-start | bytes 24580
  499.1 32.2 %copy-start.6 = (f32[2048]{0:T(1024)S(1)}, f32[2048]{0:T(1024)}, u32[]{:S(2)}) copy-start(f32[2048]{0:T(1024)} %param.22) | copy-start | bytes 24580
  499.2 57.1 %all-gather.20.cloned.1.call-start = ((), (), s32[]{:S(2)}) async-start(), calls=%async_computation.9 | async-start | bytes 2621440 | tf_op jit(solution)/shard_map/all_gather | solution.py:94
Sparse Core Ops, SparseCore 0:
  9.5 42.9 all-gather.9
  54.6 38.9 all-gather.11
  95.8 38.9 all-gather.13
  136.8 38.9 all-gather.7
  181.1 50.0 all-reduce.2
  233.2 124.5 all-gather.15
  359.9 122.6 all-gather.17
  499.3 29.3 reduce-scatter.1
  533.6 22.5 all-gather.19
where the time goes:
time: 566 us
  waiting for transfers between devices  511 us (90%)
  matrix products  26.2 us (5%)
  between operations  13.3 us (2%)
  other arithmetic  10.9 us (2%)
    all_gather x1, waiting for transfers between devices, local(): down_full = lax.all_gather(down_weight, 'fs', axis=0, tiled=True)  125 us
    all_gather x1, waiting for transfers between devices, local(): lax.all_gather(up_weight, 'fs', axis=0, tiled=True)  121 us
    psum x1, waiting for transfers between devices, local(): lax.psum(rounded_partial(conv_out, output_weight).astype(jnp.bfloat16), '...  48.7 us
    all_gather x1, waiting for transfers between devices, local(): lax.all_gather(gate_inner, 'fs', axis=0, tiled=True)  42.3 us
    all_gather x1, waiting for transfers between devices, local(): lax.all_gather(gate_outer, 'fs', axis=0, tiled=True)  41 us
    all_gather x1, waiting for transfers between devices, local(): output_weight = lax.all_gather(mixer_output, 'fs', axis=0, tiled=True)  39.2 us
    all_gather x1, waiting for transfers between devices, local(): lax.all_gather(conv_input, 'fs', axis=0, tiled=True)  38.6 us
    reduce_scatter x1, waiting for transfers between devices, local(): lax.psum_scatter(rounded_partial(hidden, down_full).astype(jnp.bfloat16),...  29.4 us
  transfers between devices with their start and end apart: 9, of which 9 were waited for; matrix products, arithmetic and copies ran while one was open for 2% of the time, Pallas kernels for 0%

commit v1 on v0

v1 whole, which is shorter than its diff:
```python
import functools

import jax
import jax.numpy as jnp
from jax import lax
from jax.experimental import pallas as pl
from jax.experimental.pallas import tpu as pltpu
from jax.sharding import PartitionSpec as P

residual_scale = 8.0**0.25
norm_epsilon = 1e-05
MESH = pl.DeviceIdType.MESH
f32 = jnp.float32
bf16 = jnp.bfloat16
NT = (((1,), (1,)), ((), ()))


def layer_norm(values, gain, shift):
    row_mean = jnp.mean(values, -1, keepdims=True)
    centered = values - row_mean
    variance = jnp.mean(centered * centered, -1, keepdims=True)
    return centered * lax.rsqrt(variance + norm_epsilon) * gain + shift


def kernel(
    n_fs,
    n_tp,
    via,
    tokens,
    w_go,
    w_gi,
    w_ci,
    w_mo,
    taps,
    m_gain,
    m_shift,
    w_up,
    w_dn,
    c_gain,
    c_shift,
    out,
    mix_g,
    up_g,
    dn_g,
    outer,
    zpad,
    conv,
    part,
    part2,
    first,
    hidden,
    result,
    recv1,
    recv2,
    local_sem,
    gs_send,
    gs_recv,
    ts_send,
    ts_recv,
):
    seq, width = tokens.shape
    rows = w_up.shape[0]
    units = w_up.shape[1]
    bits = n_tp.bit_length() - 1
    nk = n_fs // 2
    f = lax.axis_index("fs")
    t = lax.axis_index("tp")
    k = f // 2
    p = f % 2
    partner = f + 1 - 2 * p
    has_right = k < nk - 1
    has_left = k > 0

    def flip(bit):
        return t + bit - 2 * bit * ((t // bit) % 2)

    own = pl.ds(pl.multiple_of(f * rows, rows), rows)
    copies = []
    for j, ref in enumerate((w_go, w_gi, w_ci, w_mo)):
        copies.append(pltpu.make_async_copy(ref, mix_g.at[j, own], local_sem.at[j]))
    copies.append(pltpu.make_async_copy(w_up, up_g.at[own], local_sem.at[4]))
    copies.append(pltpu.make_async_copy(w_dn, dn_g.at[own], local_sem.at[5]))
    for c in copies:
        c.start()

    barrier = pltpu.get_barrier_semaphore()
    pl.semaphore_signal(barrier, inc=1, device_id={"fs": partner}, device_id_type=MESH)

    @pl.when(has_right)
    def _():
        pl.semaphore_signal(barrier, inc=1, device_id={"fs": f + 2}, device_id_type=MESH)

    @pl.when(has_left)
    def _():
        pl.semaphore_signal(barrier, inc=1, device_id={"fs": f - 2}, device_id_type=MESH)

    for b in range(bits):
        pl.semaphore_signal(barrier, inc=1, device_id={"tp": flip(1 << b)}, device_id_type=MESH)
    neighbours = (k + nk - 1) // nk + (2 * nk - 2 - k) // nk
    pl.semaphore_wait(barrier, 1 + bits + neighbours)

    for c in copies:
        c.wait()

    bufs = (mix_g, up_g, dn_g)
    spans = ((0, rows - via), (rows - via, via))

    def piece(a, s, q):
        lo, n = spans[q]
        at = pl.ds(pl.multiple_of(s * rows + lo, 16), n)
        return bufs[a].at[:, at] if a == 0 else bufs[a].at[at]

    def copy(a, s, q, way):
        target = (partner, f + 2, f - 2)[way]
        ref = piece(a, s, q)
        return pltpu.make_async_remote_copy(
            src_ref=ref,
            dst_ref=ref,
            send_sem=gs_send.at[a, s, q, way],
            recv_sem=gs_recv.at[a, s, q],
            device_id={"fs": target},
            device_id_type=MESH,
        )

    def send(a, s, q, way):
        if way == 0:
            copy(a, s, q, 0).start()
        else:

            @pl.when(has_right if way == 1 else has_left)
            def _():
                copy(a, s, q, way).start()

    def arrive(a, s, q):
        copy(a, s, q, 0).wait_recv()

    def begin(a):
        for q in (0, 1):
            for way in (0, 1, 2):
                send(a, f, q, way)

    def after_pair(a):
        arrive(a, partner, 0)
        send(a, partner, 0, 1)
        send(a, partner, 0, 2)

    def step(a, d):
        for way, s, ok in ((1, f - 2 * d, k - d >= 0), (2, f + 2 * d, k + d < nk)):

            @pl.when(ok)
            def _(way=way, s=s):
                other = s + 1 - 2 * p
                for q in (1, 0):
                    arrive(a, s, q)
                    if q == 1:
                        send(a, s, q, 0)
                    send(a, s, q, way)
                arrive(a, other, 0)
                send(a, other, 0, way)

    def finish(a):
        arrive(a, partner, 1)
        for d in range(1, nk):
            for s, ok in ((f - 2 * d, k - d >= 0), (f + 2 * d, k + d < nk)):

                @pl.when(ok)
                def _(s=s):
                    arrive(a, s + 1 - 2 * p, 1)

    def drain(a):
        for q in (0, 1):
            copy(a, f, q, 0).wait_send()
            for way, has in ((1, has_right), (2, has_left)):

                @pl.when(has)
                def _(q=q, way=way):
                    copy(a, f, q, way).wait_send()
                    if q == 0:
                        copy(a, partner, q, way).wait_send()

        for d in range(1, nk):
            for way, s, ok in ((1, f - 2 * d, k - d >= 0), (2, f + 2 * d, k + d < nk)):

                @pl.when(ok)
                def _(way=way, s=s):
                    copy(a, s, 1, 0).wait_send()

                    @pl.when(has_right if way == 1 else has_left)
                    def _():
                        copy(a, s, 0, way).wait_send()
                        copy(a, s, 1, way).wait_send()
                        copy(a, s + 1 - 2 * p, 0, way).wait_send()

    starts = [0]
    for b in range(bits):
        starts.append(starts[-1] + ((t // (1 << b)) % 2) * (seq >> (b + 1)))

    def block_rows(start, b):
        return pl.ds(pl.multiple_of(start, seq >> b), seq >> b)

    def tp_copy(kind, src, dst, b):
        return pltpu.make_async_remote_copy(
            src_ref=src,
            dst_ref=dst,
            send_sem=ts_send.at[kind, b],
            recv_sem=ts_recv.at[kind, b],
            device_id={"tp": flip(1 << b)},
            device_id_type=MESH,
        )

    def reduce_copy(kind, source, landing, b):
        n = seq >> (b + 1)
        away = starts[b] + (1 - (t // (1 << b)) % 2) * n
        base = seq - (seq >> b)
        return tp_copy(kind, source.at[block_rows(away, b + 1)], landing.at[pl.ds(base, n)], b)

    def reduce_add(source, landing, b):
        n = seq >> (b + 1)
        base = seq - (seq >> b)
        tile = min(n, 32)

        @pl.loop(0, n // tile)
        def _(i):
            mine = pl.ds(pl.multiple_of(starts[b + 1] + i * tile, tile), tile)
            theirs = pl.ds(pl.multiple_of(base + i * tile, tile), tile)
            source[mine] = (source[mine].astype(f32) + landing[theirs].astype(f32)).astype(bf16)

    def gather_copy(kind, buf, b):
        ref = buf.at[block_rows(starts[b + 1], b + 1)]
        return tp_copy(kind, ref, ref, b)

    def norm_own(residual, source, landing, gain, shift, dest):
        b = bits - 1
        n = seq >> bits
        base = seq - (seq >> b)
        tile = min(n, 16)

        @pl.loop(0, n // tile)
        def _(i):
            mine = pl.ds(pl.multiple_of(starts[bits] + i * tile, tile), tile)
            theirs = pl.ds(pl.multiple_of(base + i * tile, tile), tile)
            total = source[mine].astype(f32) + landing[theirs].astype(f32)
            dest[mine] = layer_norm(
                residual_scale * residual[mine].astype(f32) + total, gain[...], shift[...]
            ).astype(bf16)

    begin(0)
    after_pair(0)
    for d in range(1, nk):
        step(0, d)
    begin(1)
    finish(0)

    pad = zpad.shape[0] - seq
    zpad[0:pad] = jnp.zeros((pad, zpad.shape[1]), f32)
    tile = seq // 2

    @pl.loop(0, 2)
    def _(i):
        at = pl.ds(pl.multiple_of(i * tile, tile), tile)
        x = tokens[at]
        outer[at] = jnp.dot(x, mix_g[0], preferred_element_type=f32)
        inner = jnp.dot(x, mix_g[1], preferred_element_type=f32)
        values = jnp.dot(x, mix_g[2], preferred_element_type=f32)
        zpad[pl.ds(pl.multiple_of(i * tile + pad, 8), tile)] = inner * values

    n_taps = taps.shape[0]
    acc = jnp.zeros((seq, zpad.shape[1]), f32)
    for j in range(n_taps):
        lo = pad - (n_taps - 1) + j
        acc = acc + taps[j : j + 1] * zpad[lo : lo + seq]
    conv[...] = (outer[...] * acc).astype(bf16)
    wide = min(256, width)

    @pl.loop(0, width // wide)
    def _(i):
        at = pl.ds(pl.multiple_of(i * wide, wide), wide)
        part[:, at] = lax.dot_general(
            conv[...], mix_g[3, at], NT, preferred_element_type=f32
        ).astype(bf16)

    stages = []
    for b in range(bits):
        c = reduce_copy(0, part, recv1, b)
        stages.append(c.start)
        if b < bits - 1:
            stages.append(lambda c=c, b=b: (c.wait_recv(), reduce_add(part, recv1, b)))
        else:
            stages.append(
                lambda c=c: (
                    c.wait_recv(),
                    norm_own(tokens, part, recv1, m_gain, m_shift, first),
                )
            )
    for b in reversed(range(bits)):
        c = gather_copy(1, first, b)
        stages.append(c.start)
        stages.append(c.wait_recv)
    groups = [stages[:1]]
    for i in range(1, len(stages) - 1, 2):
        groups.append(stages[i : i + 2])
    groups.append(stages[-1:])

    def run(group):
        for g in group:
            g()

    run(groups.pop(0))
    after_pair(1)
    for d in range(1, nk):
        if groups:
            run(groups.pop(0))
        step(1, d)
    begin(2)
    while groups:
        run(groups.pop(0))
    finish(1)
    after_pair(2)

    wide_u = min(256, units)

    @pl.loop(0, units // wide_u)
    def _(i):
        at = pl.ds(pl.multiple_of(i * wide_u, wide_u), wide_u)
        u = jnp.maximum(jnp.dot(first[...], up_g[:, at], preferred_element_type=f32), 0.0)
        hidden[:, at] = (u * u).astype(bf16)

    for d in range(1, nk):
        step(2, d)
    finish(2)

    @pl.loop(0, width // wide)
    def _(i):
        at = pl.ds(pl.multiple_of(i * wide, wide), wide)
        part2[:, at] = lax.dot_general(
            hidden[...], dn_g[at], NT, preferred_element_type=f32
        ).astype(bf16)

    for b in range(bits):
        c = reduce_copy(2, part2, recv2, b)
        c.start()
        c.wait_recv()
        if b < bits - 1:
            reduce_add(part2, recv2, b)
        else:
            norm_own(first, part2, recv2, c_gain, c_shift, result)
    for b in reversed(range(bits)):
        c = gather_copy(3, result, b)
        c.start()
        c.wait_recv()
    done = pltpu.make_async_copy(result, out, local_sem.at[6])
    done.start()

    for a in range(3):
        drain(a)
    for b in range(bits):
        reduce_copy(0, part, recv1, b).wait_send()
        gather_copy(1, first, b).wait_send()
        reduce_copy(2, part2, recv2, b).wait_send()
        gather_copy(3, result, b).wait_send()
    done.wait()


def local(
    tokens,
    gate_outer,
    gate_inner,
    conv_input,
    mixer_output,
    conv_taps,
    mixer_gain,
    mixer_shift,
    up_weight,
    down_weight,
    channel_gain,
    channel_shift,
):
    seq, width = tokens.shape
    rows, units = up_weight.shape
    chans = gate_outer.shape[1]
    n_fs = lax.axis_size("fs")
    n_tp = lax.axis_size("tp")
    bits = n_tp.bit_length() - 1
    via = max(16, rows * 13 // 16 // 16 * 16)
    vmem = pl.BlockSpec(memory_space=pltpu.VMEM)
    return pl.pallas_call(
        functools.partial(kernel, n_fs, n_tp, via),
        out_shape=jax.ShapeDtypeStruct((seq, width), bf16),
        in_specs=[vmem] * 12,
        out_specs=pl.BlockSpec(memory_space=pl.ANY),
        scratch_shapes=[
            pltpu.VMEM((4, width, chans), bf16),
            pltpu.VMEM((width, units), bf16),
            pltpu.VMEM((width, units), bf16),
            pltpu.VMEM((seq, chans), f32),
            pltpu.VMEM((seq + 8, chans), f32),
            pltpu.VMEM((seq, chans), bf16),
            pltpu.VMEM((seq, width), bf16),
            pltpu.VMEM((seq, width), bf16),
            pltpu.VMEM((seq, width), bf16),
            pltpu.VMEM((seq, units), bf16),
            pltpu.VMEM((seq, width), bf16),
            pltpu.VMEM((seq, width), bf16),
            pltpu.VMEM((seq, width), bf16),
            pltpu.SemaphoreType.DMA((7,)),
            pltpu.SemaphoreType.DMA((3, n_fs, 2, 3)),
            pltpu.SemaphoreType.DMA((3, n_fs, 2)),
            pltpu.SemaphoreType.DMA((4, bits)),
            pltpu.SemaphoreType.DMA((4, bits)),
        ],
        compiler_params=pltpu.CompilerParams(
            collective_id=0, has_side_effects=True, vmem_limit_bytes=62 * 1024 * 1024
        ),
    )(
        tokens,
        gate_outer,
        gate_inner,
        conv_input,
        mixer_output,
        conv_taps,
        mixer_gain.reshape(1, width),
        mixer_shift.reshape(1, width),
        up_weight,
        down_weight,
        channel_gain.reshape(1, width),
        channel_shift.reshape(1, width),
    )


def solution(mesh):
    in_specs = (
        P(("rep", "fs"), None),
        P("fs", "tp"),
        P("fs", "tp"),
        P("fs", "tp"),
        P("fs", "tp"),
        P(None, "tp"),
        P(),
        P(),
        P("fs", "tp"),
        P("fs", "tp"),
        P(),
        P(),
    )
    out_specs = P(("rep", "fs"), None)
    return jax.shard_map(local, mesh=mesh, in_specs=in_specs, out_specs=out_specs, check_vma=False)
```

time: 566 us -> 260 us (0.46)
  waiting for transfers between devices: 511 us -> 0 us
  Pallas kernels: 0 us -> 257 us
  matrix products: 26.2 us -> 0 us
  between operations: 13.3 us -> 0.01 us
  other arithmetic: 10.9 us -> 0 us
    all_gather x7 -> x0, waiting for transfers between devices: 429 us -> none  [the longest x1 125 us: local(): down_full = lax.all_gather(down_weight, 'fs', axis=0, tiled=True)]
    pallas_call x0 -> x1, Pallas kernels: none -> 257 us  [local(): pl.pallas_call(functools.partial(kernel, n_fs, n_tp, via), out_shape=jax....]
    psum x1 -> x0, waiting for transfers between devices: 48.7 us -> none  [local(): lax.psum(rounded_partial(conv_out, output_weight).astype(jnp.bfloat16), '...]
    reduce_scatter x1 -> x0, waiting for transfers between devices: 29.4 us -> none  [local(): lax.psum_scatter(rounded_partial(hidden, down_full).astype(jnp.bfloat16),...]
    dot_general x4 -> x0, matrix products: 26.2 us -> none  [the longest x2 21.7 us: rounded_partial(): lax.dot_general(left, right_t, (((1,), (1,)), ((), ())), preferred_elemen...]
    reduce_sum x4 -> x0, other arithmetic: 6.18 us -> none  [the longest x2 3.79 us: layer_norm(): row_mean = jnp.mean(values, -1, keepdims=True)]
  transfers between devices with their start and end apart: 9 -> 0, of which waited for: 9 -> 0; matrix products, arithmetic and copies ran while one was open for 2% -> 0% of each run, Pallas kernels for 0% -> 0%
where the time goes in v1:
time: 260 us
  Pallas kernels  257 us (99%)
  local copies, waits for them, and re-layouts  3.16 us (1%)
    pallas_call x1, Pallas kernels, local(): pl.pallas_call(functools.partial(kernel, n_fs, n_tp, via), out_shape=jax....  257 us

profile of v1, /device:TPU:0, one launch (start us, length us, event | category | flops | bytes accessed | tf_op | source)
XLA Modules:
  0.0 260.3 jit_solution(1624074446757606992)
XLA Ops:
  0.0 257.2 %shard_map.118 = bf16[512,2048]{1,0:T(8,128)(2,1)} custom-call(bf16[512,2048]{1,0:T(8,128)(2,1)} %tokens.1, bf16[256,256]{1,0:T(8,128)(2,1)} %w_go.1, bf16[256,256]{1,0:T(8,128)(2,1)} %w_gi.1, bf16[256,256]{1,0:T(8,128)(2,1)} %w_ci.1, bf16[256,256]{1,0:T(8,128)(2,1)} %w_mo.1, f32[3,256]{1,0:T(4,128)} %taps.1, f32[1,2048]{1,0:T(1,128)} %bitcast.4, ...), custom_call_target="tpu_custom_call" | custom-call | tf_op jit(solution)/shard_map/pallas_call | solution.py:386
  257.2 3.2 %copy.14 = bf16[512,2048]{1,0:T(8,128)(2,1)} copy(bf16[512,2048]{1,0:T(8,128)(2,1)} %shard_map.118) | data formatting | bytes 4194304

commit v2 on v1

--- a/solution.py
+++ b/solution.py
@@ -57,6 +57,10 @@
     gs_recv,
     ts_send,
     ts_recv,
+    ms_send,
+    ms_recv,
+    ps_send,
+    ps_recv,
 ):
     seq, width = tokens.shape
     rows = w_up.shape[0]
@@ -68,8 +72,15 @@
     k = f // 2
     p = f % 2
     partner = f + 1 - 2 * p
+    e = k % 2
+    mate = f + 2 - 4 * e
+    half = units // 2
+    mine_off = e * seq
+    mate_off = (1 - e) * seq
     has_right = k < nk - 1
     has_left = k > 0
+    has_right2 = k < nk - 2
+    has_left2 = k > 1
 
     def flip(bit):
         return t + bit - 2 * bit * ((t // bit) % 2)
@@ -78,8 +89,10 @@
     copies = []
     for j, ref in enumerate((w_go, w_gi, w_ci, w_mo)):
         copies.append(pltpu.make_async_copy(ref, mix_g.at[j, own], local_sem.at[j]))
-    copies.append(pltpu.make_async_copy(w_up, up_g.at[own], local_sem.at[4]))
-    copies.append(pltpu.make_async_copy(w_dn, dn_g.at[own], local_sem.at[5]))
+    keep_cols = pl.ds(pl.multiple_of(e * half, half), half)
+    away_cols = pl.ds(pl.multiple_of((1 - e) * half, half), half)
+    for j, (w, g) in enumerate(((w_up, up_g), (w_dn, dn_g))):
+        copies.append(pltpu.make_async_copy(w.at[:, keep_cols], g.at[own], local_sem.at[4 + j]))
     for c in copies:
         c.start()
 
@@ -94,21 +107,29 @@
     def _():
         pl.semaphore_signal(barrier, inc=1, device_id={"fs": f - 2}, device_id_type=MESH)
 
+    @pl.when(has_right2)
+    def _():
+        pl.semaphore_signal(barrier, inc=1, device_id={"fs": f + 4}, device_id_type=MESH)
+
+    @pl.when(has_left2)
+    def _():
+        pl.semaphore_signal(barrier, inc=1, device_id={"fs": f - 4}, device_id_type=MESH)
+
     for b in range(bits):
         pl.semaphore_signal(barrier, inc=1, device_id={"tp": flip(1 << b)}, device_id_type=MESH)
     neighbours = (k + nk - 1) // nk + (2 * nk - 2 - k) // nk
+    neighbours += (k + nk - 2) // nk + (2 * nk - 3 - k) // nk
     pl.semaphore_wait(barrier, 1 + bits + neighbours)
 
     for c in copies:
         c.wait()
 
-    bufs = (mix_g, up_g, dn_g)
     spans = ((0, rows - via), (rows - via, via))
 
     def piece(a, s, q):
         lo, n = spans[q]
         at = pl.ds(pl.multiple_of(s * rows + lo, 16), n)
-        return bufs[a].at[:, at] if a == 0 else bufs[a].at[at]
+        return mix_g.at[:, at]
 
     def copy(a, s, q, way):
         target = (partner, f + 2, f - 2)[way]
@@ -191,12 +212,69 @@
                         copy(a, s, 1, way).wait_send()
                         copy(a, s + 1 - 2 * p, 0, way).wait_send()
 
+    def half_copy(a, s, way):
+        w, g = ((w_up, up_g), (w_dn, dn_g))[a]
+        dst = g.at[pl.ds(pl.multiple_of(s * rows, rows), rows)]
+        src = w.at[:, away_cols] if way > 2 else dst
+        return pltpu.make_async_remote_copy(
+            src_ref=src,
+            dst_ref=dst,
+            send_sem=ms_send.at[a, s, way],
+            recv_sem=ms_recv.at[a, s],
+            device_id={"fs": (partner, f + 4, f - 4, f + 2, f - 2)[way]},
+            device_id_type=MESH,
+        )
+
+    exists = (None, has_right2, has_left2, has_right, has_left)
+
+    def half_each(a, s, ways, act):
+        for way in ways:
+            if way == 0:
+                act(half_copy(a, s, way))
+            else:
+
+                @pl.when(exists[way])
+                def _(way=way):
+                    act(half_copy(a, s, way))
+
+    def half_begin(a):
+        half_each(a, f, (3, 4, 1, 2, 0), lambda c: c.start())
+
+    def half_sides(d):
+        return ((1, f - 2 * d, k - d >= 0), (2, f + 2 * d, k + d < nk))
+
+    def half_step(a, d):
+        for way, s, ok in half_sides(d):
+
+            @pl.when(ok)
+            def _(way=way, s=s):
+                half_copy(a, s, 0).wait_recv()
+                half_each(a, s, (way, 0), lambda c: c.start())
+
+    def half_finish(a):
+        half_copy(a, partner, 0).wait_recv()
+        for d in range(1, nk):
+            for way, s, ok in half_sides(d):
+
+                @pl.when(ok)
+                def _(s=s):
+                    half_copy(a, s + 1 - 2 * p, 0).wait_recv()
+
+    def half_drain(a):
+        half_each(a, f, (0, 1, 2, 3, 4), lambda c: c.wait_send())
+        for d in range(1, nk):
+            for way, s, ok in half_sides(d):
+
+                @pl.when(ok)
+                def _(way=way, s=s):
+                    half_each(a, s, (way, 0), lambda c: c.wait_send())
+
     starts = [0]
     for b in range(bits):
         starts.append(starts[-1] + ((t // (1 << b)) % 2) * (seq >> (b + 1)))
 
-    def block_rows(start, b):
-        return pl.ds(pl.multiple_of(start, seq >> b), seq >> b)
+    def block_rows(start, b, off=0):
+        return pl.ds(pl.multiple_of(off + start, seq >> b), seq >> b)
 
     def tp_copy(kind, src, dst, b):
         return pltpu.make_async_remote_copy(
@@ -208,47 +286,65 @@
             device_id_type=MESH,
         )
 
-    def reduce_copy(kind, source, landing, b):
+    def reduce_copy(kind, source, landing, b, off=0, land=0):
         n = seq >> (b + 1)
         away = starts[b] + (1 - (t // (1 << b)) % 2) * n
-        base = seq - (seq >> b)
-        return tp_copy(kind, source.at[block_rows(away, b + 1)], landing.at[pl.ds(base, n)], b)
-
-    def reduce_add(source, landing, b):
-        n = seq >> (b + 1)
-        base = seq - (seq >> b)
-        tile = min(n, 32)
+        base = land + seq - (seq >> b)
+        return tp_copy(
+            kind, source.at[block_rows(away, b + 1, off)], landing.at[pl.ds(base, n)], b
+        )
+
+    def add_rows(source, start, landing, base, n):
+        tile = min(n, 16)
 
         @pl.loop(0, n // tile)
         def _(i):
-            mine = pl.ds(pl.multiple_of(starts[b + 1] + i * tile, tile), tile)
+            mine = pl.ds(pl.multiple_of(start + i * tile, tile), tile)
             theirs = pl.ds(pl.multiple_of(base + i * tile, tile), tile)
             source[mine] = (source[mine].astype(f32) + landing[theirs].astype(f32)).astype(bf16)
 
-    def gather_copy(kind, buf, b):
-        ref = buf.at[block_rows(starts[b + 1], b + 1)]
+    def reduce_add(source, landing, b, off=0, land=0):
+        add_rows(source, off + starts[b + 1], landing, land + seq - (seq >> b), seq >> (b + 1))
+
+    def gather_copy(kind, buf, b, off=0):
+        ref = buf.at[block_rows(starts[b + 1], b + 1, off)]
         return tp_copy(kind, ref, ref, b)
 
-    def norm_own(residual, source, landing, gain, shift, dest):
-        b = bits - 1
+    def pair_copy(i, src, dst, to_mate):
+        return pltpu.make_async_remote_copy(
+            src_ref=src,
+            dst_ref=dst,
+            send_sem=ps_send.at[i],
+            recv_sem=ps_recv.at[i],
+            device_id={"fs": mate} if to_mate else {"tp": flip(1)},
+            device_id_type=MESH,
+        )
+
+    def norm_own(residual, source, landing, gain, shift, dest, off_r, off_s, land, off_d):
         n = seq >> bits
-        base = seq - (seq >> b)
+        base = land + seq - (seq >> (bits - 1))
         tile = min(n, 16)
 
         @pl.loop(0, n // tile)
         def _(i):
-            mine = pl.ds(pl.multiple_of(starts[bits] + i * tile, tile), tile)
+            at = starts[bits] + i * tile
+
+            def rows_at(off):
+                return pl.ds(pl.multiple_of(off + at, tile), tile)
+
             theirs = pl.ds(pl.multiple_of(base + i * tile, tile), tile)
-            total = source[mine].astype(f32) + landing[theirs].astype(f32)
-            dest[mine] = layer_norm(
-                residual_scale * residual[mine].astype(f32) + total, gain[...], shift[...]
+            total = source[rows_at(off_s)].astype(f32) + landing[theirs].astype(f32)
+            dest[rows_at(off_d)] = layer_norm(
+                residual_scale * residual[rows_at(off_r)].astype(f32) + total,
+                gain[...],
+                shift[...],
             ).astype(bf16)
 
     begin(0)
     after_pair(0)
     for d in range(1, nk):
         step(0, d)
-    begin(1)
+    half_begin(0)
     finish(0)
 
     pad = zpad.shape[0] - seq
@@ -289,13 +385,24 @@
             stages.append(
                 lambda c=c: (
                     c.wait_recv(),
-                    norm_own(tokens, part, recv1, m_gain, m_shift, first),
+                    norm_own(tokens, part, recv1, m_gain, m_shift, first, 0, 0, 0, mine_off),
                 )
             )
-    for b in reversed(range(bits)):
-        c = gather_copy(1, first, b)
+    n0 = seq // 2
+    for b in reversed(range(1, bits)):
+        c = gather_copy(1, first, b, mine_off)
         stages.append(c.start)
         stages.append(c.wait_recv)
+    held = first.at[block_rows(starts[1], 1, mine_off)]
+    to_mate = pair_copy(0, held, held, True)
+    stages.append(to_mate.start)
+    stages.append(to_mate.wait_recv)
+    across = []
+    for q in (0, 1):
+        ref = first.at[block_rows(starts[1], 1, q * seq)]
+        across.append(pair_copy(1 + q, ref, ref, False))
+    stages.append(lambda: [c.start() for c in across])
+    stages.append(lambda: [c.wait_recv() for c in across])
     groups = [stages[:1]]
     for i in range(1, len(stages) - 1, 2):
         groups.append(stages[i : i + 2])
@@ -306,28 +413,27 @@
             g()
 
     run(groups.pop(0))
-    after_pair(1)
     for d in range(1, nk):
         if groups:
             run(groups.pop(0))
-        step(1, d)
-    begin(2)
+        half_step(0, d)
+    half_begin(1)
+    half_step(1, 1)
     while groups:
         run(groups.pop(0))
-    finish(1)
-    after_pair(2)
-
-    wide_u = min(256, units)
-
-    @pl.loop(0, units // wide_u)
+    half_finish(0)
+
+    wide_u = min(256, half)
+
+    @pl.loop(0, half // wide_u)
     def _(i):
         at = pl.ds(pl.multiple_of(i * wide_u, wide_u), wide_u)
         u = jnp.maximum(jnp.dot(first[...], up_g[:, at], preferred_element_type=f32), 0.0)
         hidden[:, at] = (u * u).astype(bf16)
 
-    for d in range(1, nk):
-        step(2, d)
-    finish(2)
+    for d in range(2, nk):
+        half_step(1, d)
+    half_finish(1)
 
     @pl.loop(0, width // wide)
     def _(i):
@@ -336,14 +442,33 @@
             hidden[...], dn_g[at], NT, preferred_element_type=f32
         ).astype(bf16)
 
-    for b in range(bits):
-        c = reduce_copy(2, part2, recv2, b)
+    over = []
+    for q in (0, 1):
+        away = (1 - t % 2) * n0
+        over.append(
+            pair_copy(
+                3 + q, part2.at[block_rows(away, 1, q * seq)], recv2.at[pl.ds(q * n0, n0)], False
+            )
+        )
+    for c in over:
+        c.start()
+    for c in over:
+        c.wait_recv()
+    add_rows(part2, mate_off + starts[1], recv2, (1 - e) * n0, n0)
+    swap = pair_copy(
+        5, part2.at[block_rows(starts[1], 1, mate_off)], recv2.at[pl.ds(seq, n0)], True
+    )
+    swap.start()
+    add_rows(part2, mine_off + starts[1], recv2, e * n0, n0)
+    swap.wait_recv()
+    add_rows(part2, mine_off + starts[1], recv2, seq, n0)
+    for b in range(1, bits):
+        c = reduce_copy(2, part2, recv2, b, mine_off, seq)
         c.start()
         c.wait_recv()
         if b < bits - 1:
-            reduce_add(part2, recv2, b)
-        else:
-            norm_own(first, part2, recv2, c_gain, c_shift, result)
+            reduce_add(part2, recv2, b, mine_off, seq)
+    norm_own(first, part2, recv2, c_gain, c_shift, result, mine_off, mine_off, seq, 0)
     for b in reversed(range(bits)):
         c = gather_copy(3, result, b)
         c.start()
@@ -351,13 +476,17 @@
     done = pltpu.make_async_copy(result, out, local_sem.at[6])
     done.start()
 
-    for a in range(3):
-        drain(a)
+    drain(0)
+    half_drain(0)
+    half_drain(1)
     for b in range(bits):
         reduce_copy(0, part, recv1, b).wait_send()
-        gather_copy(1, first, b).wait_send()
-        reduce_copy(2, part2, recv2, b).wait_send()
         gather_copy(3, result, b).wait_send()
+        if b > 0:
+            gather_copy(1, first, b, mine_off).wait_send()
+            reduce_copy(2, part2, recv2, b, mine_off, seq).wait_send()
+    for c in [to_mate, swap] + across + over:
+        c.wait_send()
     done.wait()
 
 
@@ -390,23 +519,27 @@
         out_specs=pl.BlockSpec(memory_space=pl.ANY),
         scratch_shapes=[
             pltpu.VMEM((4, width, chans), bf16),
-            pltpu.VMEM((width, units), bf16),
-            pltpu.VMEM((width, units), bf16),
+            pltpu.VMEM((width, units // 2), bf16),
+            pltpu.VMEM((width, units // 2), bf16),
             pltpu.VMEM((seq, chans), f32),
             pltpu.VMEM((seq + 8, chans), f32),
             pltpu.VMEM((seq, chans), bf16),
             pltpu.VMEM((seq, width), bf16),
+            pltpu.VMEM((2 * seq, width), bf16),
+            pltpu.VMEM((2 * seq, width), bf16),
+            pltpu.VMEM((2 * seq, units // 2), bf16),
             pltpu.VMEM((seq, width), bf16),
             pltpu.VMEM((seq, width), bf16),
-            pltpu.VMEM((seq, units), bf16),
-            pltpu.VMEM((seq, width), bf16),
-            pltpu.VMEM((seq, width), bf16),
-            pltpu.VMEM((seq, width), bf16),
+            pltpu.VMEM((2 * seq, width), bf16),
             pltpu.SemaphoreType.DMA((7,)),
-            pltpu.SemaphoreType.DMA((3, n_fs, 2, 3)),
-            pltpu.SemaphoreType.DMA((3, n_fs, 2)),
+            pltpu.SemaphoreType.DMA((1, n_fs, 2, 3)),
+            pltpu.SemaphoreType.DMA((1, n_fs, 2)),
             pltpu.SemaphoreType.DMA((4, bits)),
             pltpu.SemaphoreType.DMA((4, bits)),
+            pltpu.SemaphoreType.DMA((2, n_fs, 5)),
+            pltpu.SemaphoreType.DMA((2, n_fs)),
+            pltpu.SemaphoreType.DMA((6,)),
+            pltpu.SemaphoreType.DMA((6,)),
         ],
         compiler_params=pltpu.CompilerParams(
             collective_id=0, has_side_effects=True, vmem_limit_bytes=62 * 1024 * 1024

time: 260 us -> 241 us (0.927)
  the two profiles are of different devices: /device:TPU:0 before, /device:TPU:21 now
where the time goes in v2:
time: 241 us
  Pallas kernels  238 us (99%)
  local copies, waits for them, and re-layouts  3.16 us (1%)
    pallas_call x1, Pallas kernels, local(): pl.pallas_call(functools.partial(kernel, n_fs, n_tp, via), out_shape=jax....  238 us

profile of v2, /device:TPU:21, one launch (start us, length us, event | category | flops | bytes accessed | tf_op | source)
XLA Modules:
  0.0 240.7 jit_solution(3801073151124312507)
XLA Ops:
  0.0 237.6 %shard_map.118 = bf16[512,2048]{1,0:T(8,128)(2,1)} custom-call(bf16[512,2048]{1,0:T(8,128)(2,1)} %tokens.1, bf16[256,256]{1,0:T(8,128)(2,1)} %w_go.1, bf16[256,256]{1,0:T(8,128)(2,1)} %w_gi.1, bf16[256,256]{1,0:T(8,128)(2,1)} %w_ci.1, bf16[256,256]{1,0:T(8,128)(2,1)} %w_mo.1, f32[3,256]{1,0:T(4,128)} %taps.1, f32[1,2048]{1,0:T(1,128)} %bitcast.4, ...), custom_call_target="tpu_custom_call" | custom-call | tf_op jit(solution)/shard_map/pallas_call | solution.py:515
  237.6 3.2 %copy.14 = bf16[512,2048]{1,0:T(8,128)(2,1)} copy(bf16[512,2048]{1,0:T(8,128)(2,1)} %shard_map.118) | data formatting | bytes 4194304
